TPU v7x, 768 devices: a whole 4x8x12 slice. The times are simulated.
768 devices in a mesh: sp: 384 (over z, y, x), tp: 2 (over core).
Axes of the slice: x: 4, y: 8, z: 12, core: 2. Of those that a mesh axis runs over, the one named last changes fastest.
Arguments:
- tokens: bfloat16 [98304, 2048], P('sp'), may hold values from -6 to 6
- query_weight: bfloat16 [2, 2048, 512], P(None, None, 'tp'), may hold values from -0.125 to 0.125
- key_weight: bfloat16 [2, 2048, 512], P(None, None, 'tp'), may hold values from -0.125 to 0.125
- value_weight: bfloat16 [2, 2048, 512], P(None, None, 'tp'), may hold values from -0.125 to 0.125
- out_weight: bfloat16 [2, 512, 2048], replicated, may hold values from -1.5 to 1.5
- rel_table: float32 [2, 8, 257], P(None, 'tp'), may hold values from -5 to 262
- norm_gain: float32 [2, 2048], replicated, may hold values from 0.1 to 1.9
- norm_bias: float32 [2, 2048], replicated, may hold values from -1.5 to 1.5
Outputs:
- encoded: bfloat16 [98304, 2048], P('sp', 'tp')
All inputs are finite; a program needn't handle non-finite values.
Results may differ from a plain program's by a relative error of at most 0.0095.
Values may be sent and summed in bfloat16 or wider, within the bound.
No kernel may reach another device: no remote copies, remote signals or barrier semaphores. Data moves between devices by JAX's collectives and lax.ppermute only.
A program may use at most 64 MiB of HBM per device.

v0:
```python
import jax
import jax.numpy as jnp
from jax import lax
from jax.sharding import PartitionSpec as P

SEG = 64
LEFT = 4
CLIP = 128
LAYERS = 2


residual_scale = 2.0**0.5
norm_eps = 1e-05
masked_score = -1e30


def passed_along(value, axis, steps):
    count = lax.axis_size(axis)
    initial, last = (max(0, -steps), min(count, count - steps))
    return lax.ppermute(value, axis, [(source, source + steps) for source in range(initial, last)])


def post_norm(previous, mixed, gain, shift):
    total = residual_scale * previous.astype(jnp.float32) + mixed
    mean = jnp.mean(total, -1, keepdims=True)
    centred = total - mean
    variance = jnp.mean(centred * centred, -1, keepdims=True)
    return (centred * lax.rsqrt(variance + norm_eps) * gain + shift).astype(jnp.bfloat16)


def band_bias(table, reach, band):
    head_count = table.shape[0]
    table_width = table.shape[1]
    span_count = band + SEG - 1
    offsets = jnp.arange(span_count, dtype=jnp.int32)
    distance = reach + SEG - 1 - offsets
    column = jnp.clip(distance, -CLIP, CLIP) + CLIP
    onehot = (column[None, :] == jnp.arange(table_width, dtype=jnp.int32)[:, None]).astype(
        jnp.float32
    )
    by_offset = jnp.dot(table, onehot, precision=lax.Precision.HIGHEST)
    padded = jnp.concatenate([by_offset, jnp.zeros((head_count, 1), jnp.float32)], axis=1)
    period = span_count + 1
    tiled = jnp.tile(padded, (1, SEG))
    skewed = tiled[:, SEG - 1 : SEG - 1 + SEG * (period - 1)].reshape(head_count, SEG, period - 1)
    return skewed[:, :, :band]


def attend(query, keys_ext, values_ext, table, offset):
    tok_rows = query.shape[0]
    head_count = table.shape[0]
    head_size = query.shape[1] // head_count
    seg_count = tok_rows // SEG
    reach = LEFT * SEG
    band = reach + SEG
    query_blocks = query.reshape(seg_count, SEG, head_count, head_size)
    key_blocks = keys_ext.reshape(seg_count + LEFT, SEG, head_count, head_size)
    value_blocks = values_ext.reshape(seg_count + LEFT, SEG, head_count, head_size)
    key_band = jnp.concatenate(
        [key_blocks[step : step + seg_count] for step in range(LEFT + 1)], axis=1
    )
    value_band = jnp.concatenate(
        [value_blocks[step : step + seg_count] for step in range(LEFT + 1)], axis=1
    )
    scores = jnp.einsum(
        "cqhd,ckhd->hcqk", query_blocks, key_band, preferred_element_type=jnp.float32
    )
    scores = scores * head_size ** (-0.5)
    bias = band_bias(table, reach, band)
    scores = scores + bias[:, None]
    key_position = (
        offset
        - reach
        + jnp.arange(seg_count, dtype=jnp.int32)[:, None] * SEG
        + jnp.arange(band, dtype=jnp.int32)[None, :]
    )
    scores = jnp.where((key_position >= 0)[None, :, None, :], scores, masked_score)
    peak = jnp.max(scores, -1, keepdims=True)
    expo = jnp.exp(scores - peak)
    weights = (expo / jnp.sum(expo, -1, keepdims=True)).astype(jnp.bfloat16)
    attended = jnp.einsum(
        "hcqk,ckhd->cqhd", weights, value_band, preferred_element_type=jnp.float32
    )
    return attended.astype(jnp.bfloat16).reshape(tok_rows, head_count * head_size)


def body(
    tokens, query_weight, key_weight, value_weight, out_weight, rel_table, norm_gain, norm_bias
):
    tok_rows = tokens.shape[0]
    model_width = tokens.shape[1]
    offset = lax.axis_index("sp") * tok_rows
    hidden = tokens
    for layer_index in range(LAYERS):
        query = jnp.dot(
            hidden, query_weight[layer_index], preferred_element_type=jnp.float32
        ).astype(jnp.bfloat16)
        keys = jnp.dot(hidden, key_weight[layer_index], preferred_element_type=jnp.float32).astype(
            jnp.bfloat16
        )
        values = jnp.dot(
            hidden, value_weight[layer_index], preferred_element_type=jnp.float32
        ).astype(jnp.bfloat16)
        earlier_keys, earlier_values = passed_along((keys, values), "sp", 1)
        keys_ext = jnp.concatenate([earlier_keys, keys], axis=0)
        values_ext = jnp.concatenate([earlier_values, values], axis=0)
        attended = attend(query, keys_ext, values_ext, rel_table[layer_index], offset)
        project_weight = out_weight[layer_index]
        mixed = jnp.dot(
            lax.all_gather(attended, "tp", axis=1, tiled=True),
            project_weight,
            preferred_element_type=jnp.float32,
        )
        hidden = post_norm(hidden, mixed, norm_gain[layer_index], norm_bias[layer_index])
    width = model_width // lax.axis_size("tp")
    return lax.dynamic_slice_in_dim(hidden, lax.axis_index("tp") * width, width, 1)


def solution(mesh):
    return jax.shard_map(
        body,
        mesh=mesh,
        in_specs=(
            P("sp", None),
            P(None, None, "tp"),
            P(None, None, "tp"),
            P(None, None, "tp"),
            P(),
            P(None, "tp", None),
            P(),
            P(),
        ),
        out_specs=P("sp", "tp"),
        check_vma=False,
    )
```

profile of v0, /device:TPU:513, one launch (start us, length us, event | category | flops | bytes accessed | tf_op | source)
XLA Modules:
  0.0 71.8 jit_solution(642799435007028901)
XLA Ops:
  0.0 2.1 %convolution_convert_fusion.5 = bf16[256,256]{1,0:T(8,128)(2,1)S(1)} fusion(bf16[256,2048]{1,0:T(8,128)(2,1)} %param.8, bf16[2,2048,256]{2,1,0:T(8,128)(2,1)} %param.10), kind=kOutput, calls=%fused_computation.26 | convolution fusion | flops 268500992 | bytes 2228224 | tf_op jit(solution)/shard_map/dot_general | solution.py:98
  2.1 3.1 %collective-permute-start.1 = (bf16[256,256]{1,0:T(8,128)(2,1)S(1)}, bf16[256,256]{1,0:T(8,128)(2,1)S(1)}, u32[]{:S(2)}, u32[]{:S(2)}) collective-permute-start(bf16[256,256]{1,0:T(8,128)(2,1)S(1)} %convolution_convert_fusion.5), channel_id=1, source_target_pairs={{0,2},{2,4},{4,6},{6,8},{8,10},{10,12},{12,14},{14,16},{16,18},{18... | collective-permute-start | bytes 393224 | tf_op jit(solution)/shard_map/ppermute | solution.py:20
  5.3 1.7 %convolution_convert_fusion.7 = bf16[256,256]{1,0:T(8,128)(2,1)S(1)} fusion(bf16[256,2048]{1,0:T(8,128)(2,1)} %param.8, bf16[2,2048,256]{2,1,0:T(8,128)(2,1)S(1)} %copy-done.6), kind=kOutput, calls=%fused_computation.28 | convolution fusion | flops 268500992 | bytes 2228224 | tf_op jit(solution)/shard_map/dot_general | solution.py:101
  7.0 3.1 %collective-permute-start = (bf16[256,256]{1,0:T(8,128)(2,1)S(1)}, bf16[256,256]{1,0:T(8,128)(2,1)S(1)}, u32[]{:S(2)}, u32[]{:S(2)}) collective-permute-start(bf16[256,256]{1,0:T(8,128)(2,1)S(1)} %convolution_convert_fusion.7), channel_id=1, source_target_pairs={{0,2},{2,4},{4,6},{6,8},{8,10},{10,12},{12,14},{14,16},{16,18},{18... | collective-permute-start | bytes 393224 | tf_op jit(solution)/shard_map/ppermute | solution.py:20
  10.1 0.2 convolution_bitcast_fusion.1
  10.4 0.2 convolution_bitcast_fusion
  10.7 2.0 %convolution_convert_fusion.6 = bf16[256,256]{1,0:T(8,128)(2,1)S(1)} fusion(bf16[256,2048]{1,0:T(8,128)(2,1)} %param.8, bf16[2,2048,256]{2,1,0:T(8,128)(2,1)} %param.9), kind=kOutput, calls=%fused_computation.27 | convolution fusion | flops 268500992 | bytes 2228224 | tf_op jit(solution)/shard_map/dot_general | solution.py:95
  13.2 0.2 copy.42
  13.4 0.3 copy.59
  13.7 0.3 slice.216
  14.0 1.2 %reshape.113 = f32[4,64,383]{2,1,0:T(8,128)} reshape(f32[4,24512]{1,0:T(4,128)S(1)} %slice.216) | data formatting | bytes 784384 | tf_op jit(solution)/shard_map/reshape | solution.py:45
  15.2 0.9 %reshape.112 = bf16[4,64,4,64]{3,2,1,0:T(4,128)(2,1)} reshape(bf16[256,256]{1,0:T(8,128)(2,1)S(1)} %convolution_convert_fusion.6) | data formatting | bytes 262144 | tf_op jit(solution)/shard_map/reshape | solution.py:56
  16.2 0.3 copy.60
  16.5 0.3 slice.226
  16.8 1.2 %reshape.116 = f32[4,64,383]{2,1,0:T(8,128)} reshape(f32[4,24512]{1,0:T(4,128)S(1)} %slice.226) | data formatting | bytes 784384 | tf_op jit(solution)/shard_map/reshape | solution.py:45
  18.2 0.2 copy.39
  21.1 0.6 concatenate.33
  21.7 2.9 %fusion.61 = (f32[4,4,64]{2,1,0:T(4,128)S(1)}, f32[4,4,64,320]{3,2,1,0:T(8,128)}) fusion(bf16[4,320,4,64]{1,3,0,2:T(8,128)(2,1)S(1)} %concatenate.33, f32[4,64,320]{2,1,0:T(8,128)} %bitcast.69, pred[4,320]{1,0:T(4,128)(4,1)S(1)} %add_compare_fusion, bf16[4,64,4,64]{3,2,1,0:T(4,128)(2,1)} %reshape.112), kind=kOutput, calls=%fused_computation.104 | convolution fusion | flops 43581760 | bytes 2430208 | tf_op jit(solution)/shard_map/sub | solution.py:79
  24.6 0.6 concatenate.31
  25.2 2.0 %fusion.10 = bf16[4,64,4,64]{1,3,2,0:T(8,128)(2,1)S(1)} fusion(bf16[4,320,4,64]{1,3,2,0:T(8,128)(2,1)S(1)} %concatenate.31, f32[4,4,64,320]{3,2,1,0:T(8,128)} %get-tuple-element.24, f32[4,4,64]{2,1,0:T(4,128)S(1)} %get-tuple-element.23), kind=kOutput, calls=%fused_computation.21 | convolution fusion | flops 42663936 | bytes 2101248 | tf_op jit(solution)/shard_map/hcqk,ckhd->cqhd/dot_general | solution.py:81
  27.6 2.9 %all_gather.6 = bf16[256,512]{1,0:T(8,128)(2,1)S(1)} all-gather(bf16[256,256]{1,0:T(8,128)(2,1)S(1)} %reshape.114), channel_id=1, replica_groups=mesh['sp'=384,'tp'=2] {'tp'}, dimensions={1}, use_global_device_ids=true | all-gather | bytes 393216 | tf_op jit(solution)/shard_map/all_gather | solution.py:110
  30.5 2.5 %fusion.64 = (f32[256]{0:T(256)S(1)}, f32[256,2048]{1,0:T(8,128)S(1)}) fusion(bf16[256,512]{1,0:T(8,128)(2,1)S(1)} %all_gather.6, bf16[2,512,2048]{2,1,0:T(8,128)(2,1)} %param.12, bf16[256,2048]{1,0:T(8,128)(2,1)S(1)} %copy-done.9), kind=kOutput, calls=%fused_computation.105 | convolution fusion | flops 538967808 | bytes 5506048 | tf_op jit(solution)/shard_map/dot_general | solution.py:109
  32.9 0.4 multiply_reduce_fusion.1
  33.3 0.5 add_convert_fusion
  33.8 1.1 %copy-done.5 = bf16[2,2048,256]{2,1,0:T(8,128)(2,1)S(1)} copy-done((bf16[2,2048,256]{2,1,0:T(8,128)(2,1)S(1)}, bf16[2,2048,256]{2,1,0:T(8,128)(2,1)}, u32[]{:S(2)}) %copy-start.5) | copy-done | bytes 2097176
  34.9 0.4 convolution_convert_fusion.2
  35.3 1.1 %copy-done.7 = bf16[2,2048,256]{2,1,0:T(8,128)(2,1)S(1)} copy-done((bf16[2,2048,256]{2,1,0:T(8,128)(2,1)S(1)}, bf16[2,2048,256]{2,1,0:T(8,128)(2,1)}, u32[]{:S(2)}) %copy-start.7) | copy-done | bytes 2097176
  36.5 0.4 convolution_convert_fusion.4
  36.9 2.8 %collective-permute-start.3 = (bf16[256,256]{1,0:T(8,128)(2,1)S(1)}, bf16[256,256]{1,0:T(8,128)(2,1)S(1)}, u32[]{:S(2)}, u32[]{:S(2)}) collective-permute-start(bf16[256,256]{1,0:T(8,128)(2,1)S(1)} %convolution_convert_fusion.2), channel_id=1, source_target_pairs={{0,2},{2,4},{4,6},{6,8},{8,10},{10,12},{12,14},{14,16},{16,18},{18... | collective-permute-start | bytes 393224 | tf_op jit(solution)/shard_map/ppermute | solution.py:20
  39.7 3.3 %collective-permute-start.2 = (bf16[256,256]{1,0:T(8,128)(2,1)S(1)}, bf16[256,256]{1,0:T(8,128)(2,1)S(1)}, u32[]{:S(2)}, u32[]{:S(2)}) collective-permute-start(bf16[256,256]{1,0:T(8,128)(2,1)S(1)} %convolution_convert_fusion.4), channel_id=1, source_target_pairs={{0,2},{2,4},{4,6},{6,8},{8,10},{10,12},{12,14},{14,16},{16,18},{18... | collective-permute-start | bytes 393224 | tf_op jit(solution)/shard_map/ppermute | solution.py:20
  43.1 0.4 convolution_convert_fusion.3
  43.8 0.2 copy.55
  44.1 0.9 %reshape.115 = bf16[4,64,4,64]{3,2,1,0:T(4,128)(2,1)} reshape(bf16[256,256]{1,0:T(8,128)(2,1)S(1)} %convolution_convert_fusion.3) | data formatting | bytes 262144 | tf_op jit(solution)/shard_map/reshape | solution.py:56
  45.1 3.8 %collective-permute-done.3 = bf16[256,256]{1,0:T(8,128)(2,1)S(1)} collective-permute-done((bf16[256,256]{1,0:T(8,128)(2,1)S(1)}, bf16[256,256]{1,0:T(8,128)(2,1)S(1)}, u32[]{:S(2)}, u32[]{:S(2)}) %collective-permute-start.3) | collective-permute-done | bytes 131104 | tf_op jit(solution)/shard_map/ppermute | solution.py:20
  50.6 0.9 %collective-permute-done.2 = bf16[256,256]{1,0:T(8,128)(2,1)S(1)} collective-permute-done((bf16[256,256]{1,0:T(8,128)(2,1)S(1)}, bf16[256,256]{1,0:T(8,128)(2,1)S(1)}, u32[]{:S(2)}, u32[]{:S(2)}) %collective-permute-start.2) | collective-permute-done | bytes 131104 | tf_op jit(solution)/shard_map/ppermute | solution.py:20
  51.5 0.7 %pad_maximum_fusion.1 = (bf16[256,256]{1,0:T(8,128)(2,1)}, bf16[256,256]{1,0:T(8,128)(2,1)S(1)}, bf16[256,256]{1,0:T(8,128)(2,1)}) fusion(bf16[256,256]{1,0:T(8,128)(2,1)S(1)} %convolution_convert_fusion.4, bf16[256,256]{1,0:T(8,128)(2,1)S(1)} %collective-permute-done.2), kind=kLoop, calls=%fused_computation.82 | loop fusion | flops 786432 | bytes 655360 | tf_op jit(solution)/shard_map/concatenate | solution.py:106
  52.5 1.1 %slice.188 = bf16[4,64,4,64]{3,2,1,0:T(4,128)(2,1)S(1)} reshape(bf16[256,256]{1,0:T(8,128)(2,1)} %get-tuple-element.12) | data formatting | bytes 262144 | tf_op jit(solution)/shard_map/slice | solution.py:63
  53.8 1.1 %slice.190 = bf16[4,64,4,64]{3,2,1,0:T(4,128)(2,1)S(1)} reshape(bf16[256,256]{1,0:T(8,128)(2,1)} %get-tuple-element.10) | data formatting | bytes 262144 | tf_op jit(solution)/shard_map/slice | solution.py:63
  54.9 0.9 %copy.49 = bf16[4,64,4,64]{1,3,2,0:T(8,128)(2,1)} copy(bf16[4,64,4,64]{3,2,1,0:T(4,128)(2,1)S(1)} %slice.190) | data formatting | bytes 262144 | tf_op jit(solution)/shard_map/slice | solution.py:63
  56.0 0.9 %copy.46 = bf16[4,64,4,64]{1,3,2,0:T(8,128)(2,1)} copy(bf16[4,64,4,64]{3,2,1,0:T(4,128)(2,1)S(1)} %slice.184) | data formatting | bytes 262144 | tf_op jit(solution)/shard_map/slice | solution.py:63
  56.9 1.3 %concatenate.38 = bf16[4,320,4,64]{1,3,0,2:T(8,128)(2,1)} concatenate(bf16[4,64,4,64]{1,3,0,2:T(8,128)(2,1)S(1)} %copy.51, bf16[4,64,4,64]{1,3,0,2:T(8,128)(2,1)S(1)} %copy.52, bf16[4,64,4,64]{1,3,0,2:T(8,128)(2,1)S(1)} %copy.53, bf16[4,64,4,64]{1,3,0,2:T(8,128)(2,1)S(1)} %copy.54, bf16[4,64,4,64]{1,3,0,2:T(8,128)(2,1)S(1)} %copy.55), dimensions={1} | concatenate | bytes 1310720 | tf_op jit(solution)/shard_map/concatenate | solution.py:59
  58.2 3.7 %fusion.65 = (f32[4,4,64]{2,1,0:T(4,128)}, f32[4,4,64,320]{3,2,1,0:T(8,128)}) fusion(bf16[4,320,4,64]{1,3,0,2:T(8,128)(2,1)} %concatenate.38, f32[4,64,320]{2,1,0:T(8,128)S(1)} %bitcast.68, pred[4,320]{1,0:T(4,128)(4,1)S(1)} %add_compare_fusion, bf16[4,64,4,64]{3,2,1,0:T(4,128)(2,1)} %reshape.115), kind=kOutput, calls=%fused_computation.106 | convolution fusion | flops 43581760 | bytes 2430208 | tf_op jit(solution)/shard_map/sub | solution.py:79
  61.8 0.6 concatenate.36
  62.5 1.9 %fusion.11 = bf16[4,64,4,64]{1,3,2,0:T(8,128)(2,1)S(1)} fusion(bf16[4,320,4,64]{1,3,2,0:T(8,128)(2,1)S(1)} %concatenate.36, f32[4,4,64,320]{3,2,1,0:T(8,128)} %get-tuple-element.28, f32[4,4,64]{2,1,0:T(4,128)S(1)} %copy-done.11), kind=kOutput, calls=%fused_computation.22 | convolution fusion | flops 42663936 | bytes 2101248 | tf_op jit(solution)/shard_map/hcqk,ckhd->cqhd/dot_general | solution.py:81
  64.9 3.1 %all_gather.7 = bf16[256,512]{1,0:T(8,128)(2,1)S(1)} all-gather(bf16[256,256]{1,0:T(8,128)(2,1)S(1)} %reshape.117), channel_id=1, replica_groups=mesh['sp'=384,'tp'=2] {'tp'}, dimensions={1}, use_global_device_ids=true | all-gather | bytes 393216 | tf_op jit(solution)/shard_map/all_gather | solution.py:110
  68.0 2.4 %fusion.68 = (f32[256]{0:T(256)S(1)}, f32[256,2048]{1,0:T(8,128)S(1)}) fusion(bf16[256,512]{1,0:T(8,128)(2,1)S(1)} %all_gather.7, bf16[2,512,2048]{2,1,0:T(8,128)(2,1)} %param.12, bf16[256,2048]{1,0:T(8,128)(2,1)S(1)} %add_convert_fusion), kind=kOutput, calls=%fused_computation.107 | convolution fusion | flops 538967808 | bytes 5506048 | tf_op jit(solution)/shard_map/dot_general | solution.py:109
  70.4 0.4 multiply_reduce_fusion
  70.8 1.0 %fusion.14 = bf16[256,1024]{1,0:T(8,128)(2,1)} fusion(f32[256,2048]{1,0:T(8,128)S(1)} %get-tuple-element.6, s32[]{:T(128)S(6)} %select_n.12, f32[1024]{0:T(1024)S(1)} %dynamic-slice.1, f32[1024]{0:T(1024)S(1)} %dynamic-slice, f32[256]{0:T(256)S(1)} %add_rsqrt_fusion), kind=kLoop, calls=%fused_computation.34 | loop fusion | flops 1048576 | bytes 1582084 | tf_op jit(solution)/shard_map/convert_element_type | solution.py:28
  (79 shorter events, 7.3 us)
Async XLA Ops:
  0.0 5.3 %copy-start.6 = (bf16[2,2048,256]{2,1,0:T(8,128)(2,1)S(1)}, bf16[2,2048,256]{2,1,0:T(8,128)(2,1)}, u32[]{:S(2)}) copy-start(bf16[2,2048,256]{2,1,0:T(8,128)(2,1)} %param.11) | copy-start | bytes 6291460
  0.0 10.1 %copy-start.10 = (f32[2,4,257]{2,1,0:T(4,128)S(1)}, f32[2,4,257]{2,1,0:T(4,128)}, u32[]{:S(2)}) copy-start(f32[2,4,257]{2,1,0:T(4,128)} %param.13) | copy-start | bytes 24676
  2.1 15.8 %collective-permute-start.1 = (bf16[256,256]{1,0:T(8,128)(2,1)S(1)}, bf16[256,256]{1,0:T(8,128)(2,1)S(1)}, u32[]{:S(2)}, u32[]{:S(2)}) collective-permute-start(bf16[256,256]{1,0:T(8,128)(2,1)S(1)} %convolution_convert_fusion.5), channel_id=1, source_target_pairs={{0,2},{2,4},{4,6},{6,8},{8,10},{10,12},{12,14},{14,16},{16,18},{18... | collective-permute-start | bytes 393224 | tf_op jit(solution)/shard_map/ppermute | solution.py:20
  6.9 5.7 %copy-start.3 = (f32[2,2048]{1,0:T(2,128)S(1)}, f32[2,2048]{1,0:T(2,128)}, u32[]{:S(2)}) copy-start(f32[2,2048]{1,0:T(2,128)} %param.14) | copy-start | bytes 49156
  7.0 5.7 %copy-start.4 = (f32[2,2048]{1,0:T(2,128)S(1)}, f32[2,2048]{1,0:T(2,128)}, u32[]{:S(2)}) copy-start(f32[2,2048]{1,0:T(2,128)} %param.15) | copy-start | bytes 49156
  7.0 12.6 %collective-permute-start = (bf16[256,256]{1,0:T(8,128)(2,1)S(1)}, bf16[256,256]{1,0:T(8,128)(2,1)S(1)}, u32[]{:S(2)}, u32[]{:S(2)}) collective-permute-start(bf16[256,256]{1,0:T(8,128)(2,1)S(1)} %convolution_convert_fusion.7), channel_id=1, source_target_pairs={{0,2},{2,4},{4,6},{6,8},{8,10},{10,12},{12,14},{14,16},{16,18},{18... | collective-permute-start | bytes 393224 | tf_op jit(solution)/shard_map/ppermute | solution.py:20
  25.2 5.3 %copy-start.9 = (bf16[256,2048]{1,0:T(8,128)(2,1)S(1)}, bf16[256,2048]{1,0:T(8,128)(2,1)}, u32[]{:S(2)}) copy-start(bf16[256,2048]{1,0:T(8,128)(2,1)} %param.8) | copy-start | bytes 3145732
  33.3 1.6 %copy-start.5 = (bf16[2,2048,256]{2,1,0:T(8,128)(2,1)S(1)}, bf16[2,2048,256]{2,1,0:T(8,128)(2,1)}, u32[]{:S(2)}) copy-start(bf16[2,2048,256]{2,1,0:T(8,128)(2,1)} %param.10) | copy-start | bytes 6291460
  34.9 1.6 %copy-start.7 = (bf16[2,2048,256]{2,1,0:T(8,128)(2,1)S(1)}, bf16[2,2048,256]{2,1,0:T(8,128)(2,1)}, u32[]{:S(2)}) copy-start(bf16[2,2048,256]{2,1,0:T(8,128)(2,1)} %param.11) | copy-start | bytes 6291460
  34.9 8.2 %copy-start.8 = (bf16[2,2048,256]{2,1,0:T(8,128)(2,1)S(1)}, bf16[2,2048,256]{2,1,0:T(8,128)(2,1)}, u32[]{:S(2)}) copy-start(bf16[2,2048,256]{2,1,0:T(8,128)(2,1)} %param.9) | copy-start | bytes 6291460
  36.9 12.0 %collective-permute-start.3 = (bf16[256,256]{1,0:T(8,128)(2,1)S(1)}, bf16[256,256]{1,0:T(8,128)(2,1)S(1)}, u32[]{:S(2)}, u32[]{:S(2)}) collective-permute-start(bf16[256,256]{1,0:T(8,128)(2,1)S(1)} %convolution_convert_fusion.2), channel_id=1, source_target_pairs={{0,2},{2,4},{4,6},{6,8},{8,10},{10,12},{12,14},{14,16},{16,18},{18... | collective-permute-start | bytes 393224 | tf_op jit(solution)/shard_map/ppermute | solution.py:20
  39.7 11.7 %collective-permute-start.2 = (bf16[256,256]{1,0:T(8,128)(2,1)S(1)}, bf16[256,256]{1,0:T(8,128)(2,1)S(1)}, u32[]{:S(2)}, u32[]{:S(2)}) collective-permute-start(bf16[256,256]{1,0:T(8,128)(2,1)S(1)} %convolution_convert_fusion.4), channel_id=1, source_target_pairs={{0,2},{2,4},{4,6},{6,8},{8,10},{10,12},{12,14},{14,16},{16,18},{18... | collective-permute-start | bytes 393224 | tf_op jit(solution)/shard_map/ppermute | solution.py:20
  56.9 1.3 %copy-start.2 = (f32[4,64,383]{2,1,0:T(8,128)S(1)}, f32[4,64,383]{2,1,0:T(8,128)}, u32[]{:S(2)}) copy-start(f32[4,64,383]{2,1,0:T(8,128)} %reshape.116) | copy-start | bytes 1176580
  58.2 3.7 %copy-start = (bf16[4,64,4,64]{1,3,2,0:T(8,128)(2,1)S(1)}, bf16[4,64,4,64]{1,3,2,0:T(8,128)(2,1)}, u32[]{:S(2)}) copy-start(bf16[4,64,4,64]{1,3,2,0:T(8,128)(2,1)} %copy.49) | copy-start | bytes 393220
  58.2 3.7 %copy-start.1 = (bf16[4,64,4,64]{1,3,2,0:T(8,128)(2,1)S(1)}, bf16[4,64,4,64]{1,3,2,0:T(8,128)(2,1)}, u32[]{:S(2)}) copy-start(bf16[4,64,4,64]{1,3,2,0:T(8,128)(2,1)} %copy.46) | copy-start | bytes 393220
  61.8 0.7 copy-start.11
where the time goes:
time: 72.4 us; the launch traced here: 71.8 us
  matrix products  22.9 us (32%)
  local copies, waits for them, and re-layouts  22.1 us (31%)
  starting transfers between devices  12.4 us (17%)
  blocking collectives  6.01 us (8%)
  waiting for transfers between devices  4.7 us (6%)
  other arithmetic  3.1 us (4%)
    ppermute x4, starting transfers between devices, passed_along(): lax.ppermute(value, axis, [(source, source + steps) for source in range(i...  12.4 us
    slice x20, local copies, waits for them, and re-layouts, attend(): value_blocks[step:step + seg_count]  6.76 us
    sub x2, matrix products, attend(): expo = jnp.exp(scores - peak)  6.55 us
    all_gather x2, blocking collectives, body(): lax.all_gather(attended, 'tp', axis=1, tiled=True)  6.01 us
    dot_general x2, matrix products, body(): jnp.dot(lax.all_gather(attended, 'tp', axis=1, tiled=True), project_weigh...  4.87 us
    ppermute x4, waiting for transfers between devices, passed_along(): lax.ppermute(value, axis, [(source, source + steps) for source in range(i...  4.7 us
    dot_general x2, matrix products, attend(): jnp.einsum('hcqk,ckhd->cqhd', weights, value_band, preferred_element_type...  3.88 us
    slice x20, local copies, waits for them, and re-layouts, attend(): key_blocks[step:step + seg_count]  3.85 us
  transfers between devices with their start and end apart: 4, of which 2 were waited for; matrix products, arithmetic and copies ran while one was open for 20% of the time, Pallas kernels for 0%

commit v1 on v0

v1 whole, which is shorter than its diff:
```python
import functools

import jax
import jax.numpy as jnp
from jax import lax
from jax.experimental import pallas as pl
from jax.experimental.pallas import tpu as pltpu
from jax.sharding import PartitionSpec as P

SEG = 64
LEFT = 4
CLIP = 128
LAYERS = 2
REACH = LEFT * SEG
BAND = REACH + SEG
SPAN = 384

residual_scale = 2.0**0.5
norm_eps = 1e-05
masked_score = -1e30

VM = pl.BlockSpec(memory_space=pltpu.VMEM)
SM = pl.BlockSpec(memory_space=pltpu.SMEM)
ANY = pl.BlockSpec(memory_space=pltpu.HBM)
bf16 = jnp.bfloat16
f32 = jnp.float32


def kernel_call(body, name, outs, specs, args, scratch=(), limit=24 << 20, flops=10**9):
    return pl.pallas_call(
        body,
        name=name,
        out_shape=[jax.ShapeDtypeStruct(s, d) for s, d in outs],
        in_specs=specs,
        out_specs=[VM] * len(outs),
        scratch_shapes=scratch,
        compiler_params=pltpu.CompilerParams(vmem_limit_bytes=limit),
        cost_estimate=pl.CostEstimate(flops=flops, transcendentals=0, bytes_accessed=1 << 20),
    )(*args)


def matmul(a, b):
    return jnp.dot(a, b, preferred_element_type=f32)


def first_kv(tok, wk, wv, kv, tokv, wks, wvs, sem):
    rows, width = tok.shape
    heads = wk.shape[2]
    parts = sem.shape[1]
    step = width // parts
    copies = []
    for c in range(parts):
        cut = pl.ds(c * step, step)
        trio = (
            pltpu.make_async_copy(tok.at[:, cut], tokv.at[:, cut], sem.at[0, c]),
            pltpu.make_async_copy(wk.at[0, cut, :], wks.at[cut, :], sem.at[1, c]),
            pltpu.make_async_copy(wv.at[0, cut, :], wvs.at[cut, :], sem.at[2, c]),
        )
        for copy in trio:
            copy.start()
        copies.append(trio)
    keys = values = None
    for c in range(parts):
        for copy in copies[c]:
            copy.wait()
        cut = pl.ds(c * step, step)
        x = tokv[:, cut]
        k = matmul(x, wks[cut, :])
        v = matmul(x, wvs[cut, :])
        keys = k if keys is None else keys + k
        values = v if values is None else values + v
    kv[:, :heads] = keys.astype(bf16)
    kv[:, heads:] = values.astype(bf16)


def fill_bias(table, bias):
    rows, cols = table.shape
    t = table[...]
    head = t[:, : cols - 1]
    offset = lax.broadcasted_iota(jnp.int32, (cols - 1, SPAN), 1)
    index = lax.broadcasted_iota(jnp.int32, (cols - 1, SPAN), 0)
    onehot = (jnp.clip(REACH + SEG - 1 - offset, -CLIP, CLIP) + CLIP == index).astype(f32).astype(bf16)
    high = head.astype(bf16)
    rest = head - high.astype(f32)
    mid = rest.astype(bf16)
    low = (rest - mid.astype(f32)).astype(bf16)
    by_offset = matmul(high, onehot) + matmul(mid, onehot) + matmul(low, onehot)
    far = lax.broadcasted_iota(jnp.int32, (rows, SPAN), 1) <= REACH + SEG - 1 - CLIP
    by_offset = jnp.where(far, t[:, cols - 1 :], by_offset)
    for r in range(rows):
        line = jnp.broadcast_to(by_offset[r : r + 1, :], (SEG, SPAN))
        skew = pltpu.roll(line, SPAN - (SEG - 1), 1, stride=1, stride_axis=0)
        bias[r * SEG : (r + 1) * SEG, :] = skew


def first_query(tokv, wq, wo, wk, wv, table, q, bias, wo0, wq1, wk1, wv1, wo1, wqs, sem):
    width = tokv.shape[1]
    copies = [
        pltpu.make_async_copy(wq.at[0], wqs, sem.at[0]),
        pltpu.make_async_copy(wo.at[0], wo0, sem.at[1]),
        pltpu.make_async_copy(wk.at[1], wk1, sem.at[2]),
        pltpu.make_async_copy(wv.at[1], wv1, sem.at[3]),
        pltpu.make_async_copy(wq.at[1], wq1, sem.at[4]),
        pltpu.make_async_copy(wo.at[1], wo1, sem.at[5]),
    ]
    for copy in copies:
        copy.start()
    fill_bias(table, bias)
    copies[0].wait()
    q[...] = (matmul(tokv[...], wqs[...]).astype(bf16).astype(f32) * 0.125).astype(bf16)
    for copy in copies[1:]:
        copy.wait()


def later_query(x, wq, q):
    q[...] = (matmul(x[...], wq[...]).astype(bf16).astype(f32) * 0.125).astype(bf16)


def attention(layer, place, q, own, prev, bias, out, ext):
    rows, width = q.shape
    heads = width // 64
    ext[:rows, :] = prev[...]
    ext[rows:, :] = own[...]
    lane = lax.broadcasted_iota(jnp.int32, (SEG, width), 1) // 64
    column = lax.broadcasted_iota(jnp.int32, (1, BAND), 1)
    blocked = jnp.where(place[0] == 0, masked_score, 0.0)
    for i in range(rows // SEG):
        qs = q[i * SEG : (i + 1) * SEG, :]
        stack = jnp.concatenate(
            [jnp.where(lane == h, qs, jnp.zeros_like(qs)) for h in range(heads)], axis=0
        )
        keys = ext[i * SEG : i * SEG + BAND, :width]
        values = ext[i * SEG : i * SEG + BAND, width:]
        score = lax.dot_general(stack, keys, (((1,), (1,)), ((), ())), preferred_element_type=f32)
        score = score + bias[layer * heads * SEG : (layer + 1) * heads * SEG, :BAND]
        score = score + jnp.where(column < REACH - i * SEG, blocked, 0.0)
        peak = jnp.max(score, -1, keepdims=True)
        expo = jnp.exp(score - peak)
        scale = 1.0 / jnp.sum(expo, -1, keepdims=True)
        mixed = matmul(expo.astype(bf16), values) * scale
        total = None
        for h in range(heads):
            part = jnp.where(lane == h, mixed[h * SEG : (h + 1) * SEG, :], 0.0)
            total = part if total is None else total + part
        out[i * SEG : (i + 1) * SEG, :] = total.astype(bf16)


def out_project(att, wo, x, total):
    width = x.shape[1]
    step = 512
    a = att[...]
    acc = None
    for c in range(width // step):
        cut = slice(c * step, (c + 1) * step)
        t = residual_scale * x[:, cut].astype(f32) + matmul(a, wo[:, cut])
        total[:, cut] = t
        s = jnp.sum(t, -1, keepdims=True)
        acc = s if acc is None else acc + s
    mean = acc * (1.0 / width)
    acc = None
    for c in range(width // step):
        cut = slice(c * step, (c + 1) * step)
        d = total[:, cut] - mean
        s = jnp.sum(d * d, -1, keepdims=True)
        acc = s if acc is None else acc + s
    return mean, lax.rsqrt(acc * (1.0 / width) + norm_eps)


def middle(layer, att, wo, x, gain, shift, wk, wv, y, kv, total):
    width = x.shape[1]
    heads = wk.shape[1]
    mean, scale = out_project(att, wo, x, total)
    step = 512
    keys = values = None
    for c in range(width // step):
        cut = slice(c * step, (c + 1) * step)
        d = (total[:, cut] - mean) * scale * gain[layer : layer + 1, cut] + shift[layer : layer + 1, cut]
        d = d.astype(bf16)
        y[:, cut] = d
        k = matmul(d, wk[cut, :])
        v = matmul(d, wv[cut, :])
        keys = k if keys is None else keys + k
        values = v if values is None else values + v
    kv[:, :heads] = keys.astype(bf16)
    kv[:, heads:] = values.astype(bf16)


def last(layer, place, att, wo, x, gain, shift, out, total):
    half = out.shape[1]
    mean, scale = out_project(att, wo, x, total)
    start = pl.multiple_of(place[1] * half, 128)
    cut = pl.ds(start, half)
    g = gain[layer : layer + 1, cut]
    s = shift[layer : layer + 1, cut]
    out[...] = ((total[:, cut] - mean) * scale * g + s).astype(bf16)


def body(tokens, wq, wk, wv, wo, table, gain, shift):
    rows, width = tokens.shape
    cols = wq.shape[2]
    heads = table.shape[1]
    sp = lax.axis_index("sp")
    tp = lax.axis_index("tp")
    place = jnp.stack([sp, tp]).astype(jnp.int32)
    count = lax.axis_size("sp")
    along = [(s, s + 1) for s in range(count - 1)]
    tokens, wq, wk, wv, wo = (
        pltpu.with_memory_space_constraint(a, pltpu.HBM) for a in (tokens, wq, wk, wv, wo)
    )
    flat_table = table.reshape(LAYERS * heads, table.shape[2])

    kv, x = kernel_call(
        first_kv, "kv0", [((rows, 2 * cols), bf16), ((rows, width), bf16)], [ANY, ANY, ANY], (tokens, wk, wv),
        [pltpu.VMEM((width, cols), bf16), pltpu.VMEM((width, cols), bf16), pltpu.SemaphoreType.DMA((3, 4))],
        flops=10**8,
    )
    prev = lax.ppermute(kv, "sp", along)
    q, bias, wo0, wq1, wk1, wv1, wo1 = kernel_call(
        first_query, "q0",
        [((rows, cols), bf16), ((LAYERS * heads * SEG, SPAN), f32), (wo.shape[1:], bf16), (wq.shape[1:], bf16),
         (wq.shape[1:], bf16), (wq.shape[1:], bf16), (wo.shape[1:], bf16)],
        [VM, ANY, ANY, ANY, ANY, VM], (x, wq, wo, wk, wv, flat_table),
        [pltpu.VMEM((width, cols), bf16), pltpu.SemaphoreType.DMA((6,))],
    )
    wouts = (wo0, wo1)
    for layer in range(LAYERS):
        att = kernel_call(
            functools.partial(attention, layer), f"att{layer}", [((rows, cols), bf16)],
            [SM, VM, VM, VM, VM], (place, q, kv, prev, bias),
            [pltpu.VMEM((2 * rows, 2 * cols), bf16)],
        )[0]
        full = lax.all_gather(att, "tp", axis=1, tiled=True)
        if layer + 1 < LAYERS:
            x, kv = kernel_call(
                functools.partial(middle, layer), "mid", [((rows, width), bf16), ((rows, 2 * cols), bf16)],
                [VM] * 7, (full, wouts[layer], x, gain, shift, wk1, wv1),
                [pltpu.VMEM((rows, width), f32)], flops=10**8,
            )
            prev = lax.ppermute(kv, "sp", along)
            q = kernel_call(later_query, "q1", [((rows, cols), bf16)], [VM, VM], (x, wq1))[0]
    return kernel_call(
        functools.partial(last, LAYERS - 1), "end", [((rows, width // 2), bf16)],
        [SM] + [VM] * 5, (place, full, wouts[-1], x, gain, shift),
        [pltpu.VMEM((rows, width), f32)],
    )[0]


def solution(mesh):
    return jax.shard_map(
        body,
        mesh=mesh,
        in_specs=(
            P("sp", None),
            P(None, None, "tp"),
            P(None, None, "tp"),
            P(None, None, "tp"),
            P(),
            P(None, "tp", None),
            P(),
            P(),
        ),
        out_specs=P("sp", "tp"),
        check_vma=False,
    )
```

time: 72.4 us -> 45.3 us (0.63)
  matrix products: 22.9 us -> 0 us
  local copies, waits for them, and re-layouts: 22.1 us -> 0.03 us
  waiting for transfers between devices: 4.7 us -> 19.8 us
  Pallas kernels: 0 us -> 14.1 us
  starting transfers between devices: 12.4 us -> 5.04 us
  other arithmetic: 3.1 us -> 0.08 us
    dot_general x12 -> x0, matrix products: 16.3 us -> none  [the longest x2 4.87 us: body(): jnp.dot(lax.all_gather(attended, 'tp', axis=1, tiled=True), project_weigh...]
    ppermute x4 -> x2, waiting for transfers between devices: 4.7 us -> 19.8 us  [body(): prev = lax.ppermute(kv, 'sp', along)]
    pallas_call x0 -> x7, Pallas kernels: none -> 14.1 us  [kernel_call(): pl.pallas_call(body, name=name, out_shape=[jax.ShapeDtypeStruct(s, d) for...]
    slice x44 -> x0, local copies, waits for them, and re-layouts: 11.2 us -> none  [the longest x20 6.76 us: attend(): value_blocks[step:step + seg_count]]
    ppermute x4 -> x2, starting transfers between devices: 12.4 us -> 5.04 us  [body(): prev = lax.ppermute(kv, 'sp', along)]
    sub x2 -> x0, matrix products: 6.55 us -> none  [attend(): expo = jnp.exp(scores - peak)]
    reshape x6 -> x1, local copies, waits for them, and re-layouts: 4.58 us -> 0.01 us  [body(): flat_table = table.reshape(LAYERS * heads, table.shape[2])]
    concatenate x6 -> x0, local copies, waits for them, and re-layouts: 3.02 us -> none  [the longest x2 1.88 us: attend(): jnp.concatenate([key_blocks[step:step + seg_count] for step in range(LEFT...]
  transfers between devices with their start and end apart: 4 -> 2, of which waited for: 2 -> 2; matrix products, arithmetic and copies ran while one was open for 20% -> 0% of each run, Pallas kernels for 0% -> 10%
where the time goes in v1:
time: 45.3 us; the launch traced here: 45.2 us
  waiting for transfers between devices  19.8 us (44%)
  Pallas kernels  14.1 us (31%)
  blocking collectives  6.01 us (13%)
  starting transfers between devices  5.04 us (11%)
    ppermute x2, waiting for transfers between devices, body(): prev = lax.ppermute(kv, 'sp', along)  19.8 us
    pallas_call x7, Pallas kernels, kernel_call(): pl.pallas_call(body, name=name, out_shape=[jax.ShapeDtypeStruct(s, d) for...  14.1 us
    all_gather x2, blocking collectives, body(): full = lax.all_gather(att, 'tp', axis=1, tiled=True)  6.01 us
    ppermute x2, starting transfers between devices, body(): prev = lax.ppermute(kv, 'sp', along)  5.04 us
  transfers between devices with their start and end apart: 2, of which 2 were waited for; matrix products, arithmetic and copies ran while one was open for 0% of the time, Pallas kernels for 10%

profile of v1, /device:TPU:513, one launch (start us, length us, event | category | flops | bytes accessed | tf_op | source)
XLA Modules:
  0.0 45.2 jit_solution(16082413873277003696)
XLA Ops:
  0.0 0.0 copy-start.2
  0.0 2.3 %kv0.1 = (bf16[256,512]{1,0:T(8,128)(2,1)S(1)}, bf16[256,2048]{1,0:T(8,128)(2,1)S(1)}) custom-call(bf16[256,2048]{1,0:T(8,128)(2,1)} %tok.1, bf16[2,2048,256]{2,1,0:T(8,128)(2,1)} %wk.3, bf16[2,2048,256]{2,1,0:T(8,128)(2,1)} %wv.3), custom_call_target="tpu_custom_call" | custom-call | flops 100000000 | bytes 1048576 | tf_op jit(solution)/shard_map/kv0/pallas_call | solution.py:30
  2.3 3.1 %collective-permute-start = (bf16[256,512]{1,0:T(8,128)(2,1)S(1)}, bf16[256,512]{1,0:T(8,128)(2,1)S(1)}, u32[]{:S(2)}, u32[]{:S(2)}) collective-permute-start(bf16[256,512]{1,0:T(8,128)(2,1)S(1)} %get-tuple-element.18.own), channel_id=1, source_target_pairs={{0,2},{2,4},{4,6},{6,8},{8,10},{10,12},{12,14},{14,16},{16,18},{18... | collective-permute-start | bytes 786440 | tf_op jit(solution)/shard_map/ppermute | solution.py:217
  5.4 0.0 copy-done.2
  5.5 3.9 %q0.1 = (bf16[256,256]{1,0:T(8,128)(2,1)S(1)}, f32[512,384]{1,0:T(8,128)S(1)}, bf16[512,2048]{1,0:T(8,128)(2,1)S(1)}, bf16[2048,256]{1,0:T(8,128)(2,1)S(1)}, bf1...) custom-call(bf16[256,2048]{1,0:T(8,128)(2,1)S(1)} %get-tuple-element.16.tokv.x, ...), custom_call_target="tpu_custom_call" | custom-call | flops 1000000000 | bytes 1048576 | tf_op jit(solution)/shard_map/q0/pallas_call | solution.py:30
  9.3 0.0 copy-start
  9.3 0.0 copy-start.1
  9.4 0.1 pad_add_fusion.place
  9.4 7.4 %collective-permute-done.prev = bf16[256,512]{1,0:T(8,128)(2,1)S(1)} collective-permute-done((bf16[256,512]{1,0:T(8,128)(2,1)S(1)}, bf16[256,512]{1,0:T(8,128)(2,1)S(1)}, u32[]{:S(2)}, u32[]{:S(2)}) %collective-permute-start) | collective-permute-done | bytes 262176 | tf_op jit(solution)/shard_map/ppermute | solution.py:217
  16.8 1.6 %att0.1 = bf16[256,256]{1,0:T(8,128)(2,1)S(1)} custom-call(s32[2]{0:T(128)S(1)} %pad_add_fusion.place, bf16[256,256]{1,0:T(8,128)(2,1)S(1)} %get-tuple-element.17.q, bf16[256,512]{1,0:T(8,128)(2,1)S(1)} %get-tuple-element.18.own, bf16[256,512]{1,0:T(8,128)(2,1)S(1)} %collective-permute-done.prev, f32[512,384]{1,0:T(8,128)S(1)} %get-tuple-element.19.bias), custom_call_target="tpu_custom_call" | custom-call | flops 1000000000 | bytes 1048576 | tf_op jit(solution)/shard_map/att0/pallas_call | solution.py:30
  18.4 3.2 %all_gather.6.att = bf16[256,512]{1,0:T(8,128)(2,1)S(1)} all-gather(bf16[256,256]{1,0:T(8,128)(2,1)S(1)} %att0.1), channel_id=1, replica_groups=mesh['sp'=384,'tp'=2] {'tp'}, dimensions={1}, use_global_device_ids=true | all-gather | bytes 393216 | tf_op jit(solution)/shard_map/all_gather | solution.py:232
  21.5 0.0 copy-done
  21.5 0.0 copy-done.1
  21.5 1.8 %mid.1 = (bf16[256,2048]{1,0:T(8,128)(2,1)S(1)}, bf16[256,512]{1,0:T(8,128)(2,1)S(1)}) custom-call(bf16[256,512]{1,0:T(8,128)(2,1)S(1)} %all_gather.6.att, bf16[512,2048]{1,0:T(8,128)(2,1)S(1)} %get-tuple-element.20.wo, bf16[256,2048]{1,0:T(8,128)(2,1)S(1)} %get-tuple-element.16.tokv.x, f32[2,2048]{1,0:T(2,128)S(1)} %copy-done, f32[2,2048]{1,0:T(2,128)S(1)} %copy-done.1, ...), custom_call_target="tpu_custom_call" | custom-call | flops 100000000 | bytes 1048576 | tf_op jit(solution)/shard_map/mid/pallas_call | solution.py:30
  23.4 1.9 %collective-permute-start.1 = (bf16[256,512]{1,0:T(8,128)(2,1)S(1)}, bf16[256,512]{1,0:T(8,128)(2,1)S(1)}, u32[]{:S(2)}, u32[]{:S(2)}) collective-permute-start(bf16[256,512]{1,0:T(8,128)(2,1)S(1)} %get-tuple-element.25.own), channel_id=1, source_target_pairs={{0,2},{2,4},{4,6},{6,8},{8,10},{10,12},{12,14},{14,16},{16,18},{18... | collective-permute-start | bytes 786440 | tf_op jit(solution)/shard_map/ppermute | solution.py:239
  25.3 0.5 q1.1.q
  25.8 12.4 %collective-permute-done.1.prev = bf16[256,512]{1,0:T(8,128)(2,1)S(1)} collective-permute-done((bf16[256,512]{1,0:T(8,128)(2,1)S(1)}, bf16[256,512]{1,0:T(8,128)(2,1)S(1)}, u32[]{:S(2)}, u32[]{:S(2)}) %collective-permute-start.1) | collective-permute-done | bytes 262176 | tf_op jit(solution)/shard_map/ppermute | solution.py:239
  38.2 1.6 %att1.1 = bf16[256,256]{1,0:T(8,128)(2,1)S(1)} custom-call(s32[2]{0:T(128)S(1)} %pad_add_fusion.place, bf16[256,256]{1,0:T(8,128)(2,1)S(1)} %q1.1.q, bf16[256,512]{1,0:T(8,128)(2,1)S(1)} %get-tuple-element.25.own, bf16[256,512]{1,0:T(8,128)(2,1)S(1)} %collective-permute-done.1.prev, f32[512,384]{1,0:T(8,128)S(1)} %get-tuple-element.19.bias), custom_call_target="tpu_custom_call" | custom-call | flops 1000000000 | bytes 1048576 | tf_op jit(solution)/shard_map/att1/pallas_call | solution.py:30
  39.7 2.9 %all_gather.7.att = bf16[256,512]{1,0:T(8,128)(2,1)S(1)} all-gather(bf16[256,256]{1,0:T(8,128)(2,1)S(1)} %att1.1), channel_id=1, replica_groups=mesh['sp'=384,'tp'=2] {'tp'}, dimensions={1}, use_global_device_ids=true | all-gather | bytes 393216 | tf_op jit(solution)/shard_map/all_gather | solution.py:232
  42.6 2.6 %end.1 = bf16[256,1024]{1,0:T(8,128)(2,1)} custom-call(s32[2]{0:T(128)S(1)} %pad_add_fusion.place, bf16[256,512]{1,0:T(8,128)(2,1)S(1)} %all_gather.7.att, bf16[512,2048]{1,0:T(8,128)(2,1)S(1)} %get-tuple-element.26.wo, bf16[256,2048]{1,0:T(8,128)(2,1)S(1)} %get-tuple-element.23.x, f32[2,2048]{1,0:T(2,128)S(1)} %copy-done, f32[2,2048]{1,0:T(2,128)S(1)} %copy-done.1), custom_call_target="tpu_custom_call" | custom-call | flops 1000000000 | bytes 1048576 | tf_op jit(solution)/shard_map/end/pallas_call | solution.py:30
  (1 shorter events, 0.0 us)
Async XLA Ops:
  0.0 5.4 %copy-start.2 = (f32[2,4,257]{2,1,0:T(4,128)S(1)}, f32[2,4,257]{2,1,0:T(4,128)}, u32[]{:S(2)}) copy-start(f32[2,4,257]{2,1,0:T(4,128)} %param.13) | copy-start | bytes 24676
  2.3 14.5 %collective-permute-start = (bf16[256,512]{1,0:T(8,128)(2,1)S(1)}, bf16[256,512]{1,0:T(8,128)(2,1)S(1)}, u32[]{:S(2)}, u32[]{:S(2)}) collective-permute-start(bf16[256,512]{1,0:T(8,128)(2,1)S(1)} %get-tuple-element.18.own), channel_id=1, source_target_pairs={{0,2},{2,4},{4,6},{6,8},{8,10},{10,12},{12,14},{14,16},{16,18},{18... | collective-permute-start | bytes 786440 | tf_op jit(solution)/shard_map/ppermute | solution.py:217
  9.3 12.2 %copy-start = (f32[2,2048]{1,0:T(2,128)S(1)}, f32[2,2048]{1,0:T(2,128)}, u32[]{:S(2)}) copy-start(f32[2,2048]{1,0:T(2,128)} %gain.3) | copy-start | bytes 49156
  9.3 12.2 %copy-start.1 = (f32[2,2048]{1,0:T(2,128)S(1)}, f32[2,2048]{1,0:T(2,128)}, u32[]{:S(2)}) copy-start(f32[2,2048]{1,0:T(2,128)} %shift.3) | copy-start | bytes 49156
  23.4 14.8 %collective-permute-start.1 = (bf16[256,512]{1,0:T(8,128)(2,1)S(1)}, bf16[256,512]{1,0:T(8,128)(2,1)S(1)}, u32[]{:S(2)}, u32[]{:S(2)}) collective-permute-start(bf16[256,512]{1,0:T(8,128)(2,1)S(1)} %get-tuple-element.25.own), channel_id=1, source_target_pairs={{0,2},{2,4},{4,6},{6,8},{8,10},{10,12},{12,14},{14,16},{16,18},{18... | collective-permute-start | bytes 786440 | tf_op jit(solution)/shard_map/ppermute | solution.py:239
